TPU v7x, 32 devices: a whole 2x2x4 slice. The times are simulated.
32 devices in a mesh: grp: 2 (over x), tp: 4 (over y, core), dp: 4 (over z).
Axes of the slice: x: 2, y: 2, z: 4, core: 2. Of those that a mesh axis runs over, the one named last changes fastest.
Arguments:
- hidden_in: bfloat16 [256, 4096], P('grp', 'dp'), parts along dimension 0, may hold values from -6 to 6
- state_in: float32 [2, 256, 32, 4096], P(None, ('grp', 'dp'), 'tp'), parts along dimension 1, may hold values from -0.6 to 0.6
- w_query: bfloat16 [2, 4096, 2048], P(None, 'dp', 'tp'), may hold values from -0.09375 to 0.09375
- w_key: bfloat16 [2, 4096, 2048], P(None, 'dp', 'tp'), may hold values from -0.09375 to 0.09375
- w_value: bfloat16 [2, 4096, 2048], P(None, 'dp', 'tp'), may hold values from -0.09375 to 0.09375
- w_gate: bfloat16 [2, 4096, 2048], P(None, 'dp', 'tp'), may hold values from -0.09375 to 0.09375
- w_beta: bfloat16 [2, 4096, 32], P(None, 'dp'), may hold values from -0.09375 to 0.09375
- w_decay: bfloat16 [2, 4096, 32], P(None, 'dp'), may hold values from -0.09375 to 0.09375
- decay_rate: float32 [2, 32], P(None, 'tp'), may hold values from 0.05 to 2
- out_gain: float32 [2, 64], replicated, may hold values from 0.1 to 1.9
- w_out: bfloat16 [2, 2048, 4096], P(None, 'tp', 'dp'), may hold values from -0.0625 to 0.0625
- post_gain: float32 [2, 4096], P(None, 'dp'), may hold values from 0.1 to 1.9
- post_bias: float32 [2, 4096], P(None, 'dp'), may hold values from -1.8 to 1.8
Outputs:
- hidden_out: bfloat16 [256, 4096], P('grp', 'dp'), parts along dimension 0
- state_out: float32 [2, 256, 32, 4096], P(None, ('grp', 'dp'), 'tp'), parts along dimension 1
There are 2 independent parts, one for each index of `grp`. A program takes and returns all parts, laid end to end along the dimension named above; an argument that names none is the same for every part. Nothing has to cross between parts.
All inputs are finite; a program needn't handle non-finite values.
Results may differ from a plain program's by a relative error of at most 0.018.
Values may be sent and summed in bfloat16 or wider, within the bound.
A program may use at most 128 MiB of HBM per device.

v0:
```python
import jax
import jax.numpy as jnp
from jax import lax
from jax.sharding import PartitionSpec as P

D = 4096
HEAD_DIM = 64
LAYERS = 2


residual_scale = 2.0**0.5


def unit_norm(tensor):
    return tensor * lax.rsqrt(jnp.sum(tensor * tensor, axis=-1, keepdims=True) + 1e-06)


def delta_step(
    state_now, query_pre, key_pre, value_pre, gate_pre, beta_pre, decay_pre, decay_speed, norm_gain
):
    head_dim = query_pre.shape[-1]
    query_unit = unit_norm(query_pre.astype(jnp.float32)) * head_dim ** (-0.5)
    key_unit = unit_norm(key_pre.astype(jnp.float32))
    values_f = value_pre.astype(jnp.float32)
    beta_gate = jax.nn.sigmoid(beta_pre.astype(jnp.float32))[..., None, None]
    retain = jnp.exp(-decay_speed * jax.nn.softplus(decay_pre.astype(jnp.float32)))[..., None, None]
    matrix = state_now.reshape(state_now.shape[0], state_now.shape[1], head_dim, head_dim)
    readout = jnp.einsum("bhd,bhde->bhe", key_unit, matrix, precision=lax.Precision.HIGHEST)
    matrix = (
        retain * (matrix - beta_gate * key_unit[..., :, None] * readout[..., None, :])
        + beta_gate * key_unit[..., :, None] * values_f[..., None, :]
    )
    output_vec = jnp.einsum("bhd,bhde->bhe", query_unit, matrix, precision=lax.Precision.HIGHEST)
    output_vec = output_vec * lax.rsqrt(
        jnp.mean(output_vec * output_vec, axis=-1, keepdims=True) + 1e-05
    )
    output_vec = output_vec * norm_gain * jax.nn.silu(gate_pre.astype(jnp.float32))
    return (matrix.reshape(state_now.shape), output_vec.astype(jnp.bfloat16))


def layer_norm(combined, totals, gain_row, bias_row):
    mean_row = (totals[0] / D)[:, None]
    var_row = (totals[1] / D)[:, None] - mean_row * mean_row
    normed = (combined - mean_row) * lax.rsqrt(var_row + 1e-05)
    return (normed * gain_row + bias_row).astype(jnp.bfloat16)


def per_device(
    hidden_in,
    state_in,
    w_query,
    w_key,
    w_value,
    w_gate,
    w_beta,
    w_decay,
    decay_rate,
    out_gain,
    w_out,
    post_gain,
    post_bias,
):
    stream = hidden_in
    states = []
    heads_here = w_query.shape[2] // HEAD_DIM
    first_head = lax.axis_index("tp") * heads_here
    for block_index in range(LAYERS):
        beta_cols = lax.dynamic_slice_in_dim(w_beta[block_index], first_head, heads_here, 1)
        decay_cols = lax.dynamic_slice_in_dim(w_decay[block_index], first_head, heads_here, 1)
        part_query = jnp.dot(stream, w_query[block_index], preferred_element_type=jnp.float32)
        part_key = jnp.dot(stream, w_key[block_index], preferred_element_type=jnp.float32)
        part_value = jnp.dot(stream, w_value[block_index], preferred_element_type=jnp.float32)
        part_gate = jnp.dot(stream, w_gate[block_index], preferred_element_type=jnp.float32)
        part_beta = jnp.dot(stream, beta_cols, preferred_element_type=jnp.float32)
        part_decay = jnp.dot(stream, decay_cols, preferred_element_type=jnp.float32)
        projected = (
            lax.psum_scatter(
                part_query.astype(jnp.bfloat16), "dp", scatter_dimension=0, tiled=True
            ).astype(jnp.float32),
            lax.psum_scatter(
                part_key.astype(jnp.bfloat16), "dp", scatter_dimension=0, tiled=True
            ).astype(jnp.float32),
            lax.psum_scatter(
                part_value.astype(jnp.bfloat16), "dp", scatter_dimension=0, tiled=True
            ).astype(jnp.float32),
            lax.psum_scatter(
                part_gate.astype(jnp.bfloat16), "dp", scatter_dimension=0, tiled=True
            ).astype(jnp.float32),
            lax.psum_scatter(
                part_beta.astype(jnp.bfloat16), "dp", scatter_dimension=0, tiled=True
            ).astype(jnp.float32),
            lax.psum_scatter(
                part_decay.astype(jnp.bfloat16), "dp", scatter_dimension=0, tiled=True
            ).astype(jnp.float32),
        )
        local_rows = projected[0].shape[0]
        shaped = (local_rows, heads_here, HEAD_DIM)
        query_pre = projected[0].astype(jnp.bfloat16).reshape(shaped)
        key_pre = projected[1].astype(jnp.bfloat16).reshape(shaped)
        value_pre = projected[2].astype(jnp.bfloat16).reshape(shaped)
        gate_pre = projected[3].astype(jnp.bfloat16).reshape(shaped)
        beta_pre = projected[4].astype(jnp.bfloat16)
        decay_pre = projected[5].astype(jnp.bfloat16)
        new_state, read_vec = delta_step(
            state_in[block_index],
            query_pre,
            key_pre,
            value_pre,
            gate_pre,
            beta_pre,
            decay_pre,
            decay_rate[block_index][None, :],
            out_gain[block_index],
        )
        states.append(new_state)
        read_flat = read_vec.reshape(local_rows, heads_here * HEAD_DIM)
        out_weight = w_out[block_index]
        gathered = lax.all_gather(read_flat, "dp", axis=0, tiled=True)
        share_rows = gathered.shape[0] // lax.axis_size("tp")
        mixed_sum = lax.psum_scatter(
            jnp.dot(gathered, out_weight, preferred_element_type=jnp.float32).astype(jnp.bfloat16),
            "tp",
            scatter_dimension=0,
            tiled=True,
        ).astype(jnp.float32)
        residual = lax.dynamic_slice_in_dim(
            stream, lax.axis_index("tp") * share_rows, share_rows, 0
        )
        combined = residual_scale * residual.astype(jnp.float32) + mixed_sum
        totals = lax.psum((jnp.sum(combined, axis=1), jnp.sum(combined * combined, axis=1)), "dp")
        normed_rows = layer_norm(combined, totals, post_gain[block_index], post_bias[block_index])
        stream = lax.all_gather(normed_rows, "tp", axis=0, tiled=True)
    return (stream, jnp.stack(states, axis=0))


def solution(mesh):
    placed = (
        P("grp", "dp"),
        P(None, ("grp", "dp"), "tp", None),
        P(None, "dp", "tp"),
        P(None, "dp", "tp"),
        P(None, "dp", "tp"),
        P(None, "dp", "tp"),
        P(None, "dp", None),
        P(None, "dp", None),
        P(None, "tp"),
        P(),
        P(None, "tp", "dp"),
        P(None, "dp"),
        P(None, "dp"),
    )
    return jax.shard_map(
        per_device,
        mesh=mesh,
        in_specs=placed,
        out_specs=(P("grp", "dp"), P(None, ("grp", "dp"), "tp", None)),
        check_vma=False,
    )
```

profile of v0, /device:TPU:0, one launch (start us, length us, event | category | flops | bytes accessed | tf_op | source)
XLA Modules:
  0.0 372.5 jit_solution(6604985053476364493)
XLA Ops:
  19.9 2.3 convolution_convert_fusion.6
  23.8 7.7 %fusion.58 = (f32[1,32,8,4096]{3,2,1,0:T(8,128)}, f32[1,32,8,4096]{3,2,1,0:T(8,128)}) fusion(f32[2,32,8,4096]{3,2,1,0:T(8,128)} %param.14), kind=kLoop, calls=%fused_computation.121 | loop fusion | bytes 16777216 | tf_op jit(solution)/shard_map/slice | solution.py:105
  31.5 7.8 %reshape_squeeze.6 = f32[32,8,64,64]{3,2,1,0:T(8,128)} reshape(f32[1,32,8,4096]{3,2,1,0:T(8,128)} %get-tuple-element.17) | data formatting | bytes 8388608 | tf_op jit(solution)/shard_map/reshape;squeeze | solution.py:27
  40.2 11.7 %reduce-scatter.43.cloned.1.call-done = bf16[32,8]{1,0:T(8,128)(2,1)} async-done(((bf16[128,8]{1,0:T(8,128)(2,1)}), bf16[32,8]{1,0:T(8,128)(2,1)}) %reduce-scatter.43.cloned.1.call-update) | async-done | bytes 528
  52.8 19.0 %reduce-scatter.23.cloned.1.call-done = bf16[32,512]{1,0:T(8,128)(2,1)} async-done(((bf16[128,512]{1,0:T(8,128)(2,1)}), bf16[32,512]{1,0:T(8,128)(2,1)}) %reduce-scatter.23.cloned.1.call-update) | async-done | bytes 32784 | tf_op jit(solution)/shard_map/reduce_scatter | solution.py:77
  72.8 18.7 %reduce-scatter.25.cloned.1.call-done = bf16[32,512]{1,0:T(8,128)(2,1)} async-done(((bf16[128,512]{1,0:T(8,128)(2,1)}), bf16[32,512]{1,0:T(8,128)(2,1)}) %reduce-scatter.25.cloned.1.call-update) | async-done | bytes 32784 | tf_op jit(solution)/shard_map/reduce_scatter | solution.py:80
  92.6 9.5 %fusion.63 = f32[32,8,1,64]{3,2,1,0:T(1,128)S(1)} fusion(f32[32,8,64,1]{2,3,1,0:T(1,128)S(1)} %bitcast.118, f32[32,8,64,64]{3,2,1,0:T(8,128)} %reshape_squeeze.6), kind=kOutput, calls=%fused_computation.126 | convolution fusion | flops 12582912 | bytes 4325376 | tf_op jit(solution)/shard_map/bhd,bhde->bhe/dot_general | solution.py:28
  102.1 9.1 %reduce-scatter.27.cloned.1.call-done = bf16[32,512]{1,0:T(8,128)(2,1)} async-done(((bf16[128,512]{1,0:T(8,128)(2,1)}), bf16[32,512]{1,0:T(8,128)(2,1)}) %reduce-scatter.27.cloned.1.call-update) | async-done | bytes 32784 | tf_op jit(solution)/shard_map/reduce_scatter | solution.py:83
  112.1 10.5 %fusion.4 = f32[32,8,1,64]{3,2,1,0:T(1,128)S(1)} fusion(f32[32,8,64,1]{2,3,1,0:T(1,128)S(1)} %bitcast.124, f32[32,8,64,64]{3,2,1,0:T(8,128)} %reshape_squeeze.6, f32[32,8]{1,0:T(8,128)S(1)} %copy.21, f32[32,8,64]{2,1,0:T(8,128)S(1)} %bitcast.114, f32[32,8,64]{2,1,0:T(8,128)S(1)} %get-tuple-element.12, f32[32,8,64]{2,1,0:T(8,128)S(1)} %reshape.220), kind=kOutput, calls=%fused_computation.5 | convolution fusion | flops 17825792 | bytes 4523008 | tf_op jit(solution)/shard_map/bhd,bhde->bhe/dot_general | solution.py:33
  122.7 8.9 %reduce-scatter.29.cloned.1.call-done = bf16[32,512]{1,0:T(8,128)(2,1)} async-done(((bf16[128,512]{1,0:T(8,128)(2,1)}), bf16[32,512]{1,0:T(8,128)(2,1)}) %reduce-scatter.29.cloned.1.call-update) | async-done | bytes 32784 | tf_op jit(solution)/shard_map/reduce_scatter | solution.py:86
  132.7 13.4 %all_gather.12 = bf16[128,512]{1,0:T(8,128)(2,1)S(1)} all-gather(bf16[32,512]{1,0:T(8,128)(2,1)S(1)} %reshape.216), channel_id=1, replica_groups=mesh['grp'=2,'tp'=4,'dp'=4] {'dp'}, dimensions={0}, use_global_device_ids=true | all-gather | bytes 163840 | tf_op jit(solution)/shard_map/all_gather | solution.py:118
  148.4 18.3 %reduce-scatter.31.cloned.1.call-done = bf16[32,1024]{1,0:T(8,128)(2,1)} async-done(((bf16[128,1024]{1,0:T(8,128)(2,1)}), bf16[32,1024]{1,0:T(8,128)(2,1)}) %reduce-scatter.31.cloned.1.call-update) | async-done | bytes 65552 | tf_op jit(solution)/shard_map/reduce_scatter | solution.py:120
  167.7 11.9 %all-reduce.1 = (f32[32]{0:T(128)S(1)}, f32[32]{0:T(128)S(1)}) all-reduce(f32[32]{0:T(128)S(1)} %get-tuple-element.5, f32[32]{0:T(128)S(1)} %get-tuple-element.4), channel_id=1, replica_groups=mesh['grp'=2,'tp'=4,'dp'=4] {'dp'}, use_global_device_ids=true, to_apply=%region_13.14 | all-reduce | flops 64 | bytes 512 | tf_op jit(solution)/shard_map/psum | solution.py:130
  180.5 5.8 %all_gather.13 = bf16[128,1024]{1,0:T(8,128)(2,1)S(1)} all-gather(bf16[32,1024]{1,0:T(8,128)(2,1)S(1)} %add_convert_fusion.1), channel_id=1, replica_groups=mesh['grp'=2,'tp'=4,'dp'=4] {'tp'}, dimensions={0}, use_global_device_ids=true | all-gather | bytes 327680 | tf_op jit(solution)/shard_map/all_gather | solution.py:132
  189.3 2.3 convolution_convert_fusion.5
  191.7 7.8 %reshape_squeeze.7 = f32[32,8,64,64]{3,2,1,0:T(8,128)} reshape(f32[1,32,8,4096]{3,2,1,0:T(8,128)} %get-tuple-element.16) | data formatting | bytes 8388608 | tf_op jit(solution)/shard_map/reshape;squeeze | solution.py:27
  200.6 6.7 %broadcast_multiply_fusion.3 = (f32[32,8,64,64]{3,2,1,0:T(8,128)}, f32[32,8,64,64]{3,2,1,0:T(8,128)}) fusion(f32[32,8,64]{2,1,0:T(8,128)S(1)} %bitcast.115, f32[32,8,64]{2,1,0:T(8,128)S(1)} %get-tuple-element.12, f32[32,8,64]{2,1,0:T(8,128)S(1)} %reshape.220), kind=kLoop, calls=%fused_computation.15 | loop fusion | flops 2097152 | bytes 8585216 | tf_op jit(solution)/shard_map/mul | solution.py:30
  207.4 7.9 %mul.417 = f32[1,32,8,4096]{3,2,1,0:T(8,128)} reshape(f32[32,8,64,64]{3,2,1,0:T(8,128)} %get-tuple-element.18) | data formatting | bytes 8388608 | tf_op jit(solution)/shard_map/mul | solution.py:30
  215.3 8.1 %mul.419 = f32[1,32,8,4096]{3,2,1,0:T(8,128)} reshape(f32[32,8,64,64]{3,2,1,0:T(8,128)} %get-tuple-element.19) | data formatting | bytes 8388608 | tf_op jit(solution)/shard_map/mul | solution.py:31
  226.2 17.1 %reduce-scatter.35.cloned.1.call-done = bf16[32,512]{1,0:T(8,128)(2,1)} async-done(((bf16[128,512]{1,0:T(8,128)(2,1)}), bf16[32,512]{1,0:T(8,128)(2,1)}) %reduce-scatter.35.cloned.1.call-update) | async-done | bytes 32784 | tf_op jit(solution)/shard_map/reduce_scatter | solution.py:80
  244.3 18.9 %reduce-scatter.33.cloned.1.call-done = bf16[32,512]{1,0:T(8,128)(2,1)} async-done(((bf16[128,512]{1,0:T(8,128)(2,1)}), bf16[32,512]{1,0:T(8,128)(2,1)}) %reduce-scatter.33.cloned.1.call-update) | async-done | bytes 32784 | tf_op jit(solution)/shard_map/reduce_scatter | solution.py:77
  264.4 9.5 %fusion.64 = f32[32,8,1,64]{3,2,1,0:T(1,128)S(1)} fusion(f32[32,8,64,1]{2,3,1,0:T(1,128)S(1)} %bitcast.119, f32[32,8,64,64]{3,2,1,0:T(8,128)} %reshape_squeeze.7), kind=kOutput, calls=%fused_computation.127 | convolution fusion | flops 12582912 | bytes 4325376 | tf_op jit(solution)/shard_map/bhd,bhde->bhe/dot_general | solution.py:28
  273.9 9.1 %reduce-scatter.37.cloned.1.call-done = bf16[32,512]{1,0:T(8,128)(2,1)} async-done(((bf16[128,512]{1,0:T(8,128)(2,1)}), bf16[32,512]{1,0:T(8,128)(2,1)}) %reduce-scatter.37.cloned.1.call-update) | async-done | bytes 32784 | tf_op jit(solution)/shard_map/reduce_scatter | solution.py:83
  283.8 6.8 %broadcast_multiply_fusion.1 = (f32[32,8,64,64]{3,2,1,0:T(8,128)}, f32[32,8,64,64]{3,2,1,0:T(8,128)}) fusion(f32[32,8,64]{2,1,0:T(8,128)S(1)} %bitcast.116, f32[32,8,64]{2,1,0:T(8,128)S(1)} %get-tuple-element.10, f32[32,8,64]{2,1,0:T(8,128)S(1)} %reshape.224), kind=kLoop, calls=%fused_computation.12 | loop fusion | flops 2097152 | bytes 8585216 | tf_op jit(solution)/shard_map/mul | solution.py:30
  290.6 10.6 %fusion = f32[32,8,1,64]{3,2,1,0:T(1,128)S(1)} fusion(f32[32,8,64,1]{2,3,1,0:T(1,128)S(1)} %bitcast.125, f32[32,8,64,64]{3,2,1,0:T(8,128)} %reshape_squeeze.7, f32[32,8]{1,0:T(8,128)S(1)} %copy.23, f32[32,8,64]{2,1,0:T(8,128)S(1)} %bitcast.117, f32[32,8,64]{2,1,0:T(8,128)S(1)} %get-tuple-element.10, f32[32,8,64]{2,1,0:T(8,128)S(1)} %reshape.224), kind=kOutput, calls=%fused_computation.1 | convolution fusion | flops 17825792 | bytes 4523008 | tf_op jit(solution)/shard_map/bhd,bhde->bhe/dot_general | solution.py:33
  304.5 13.6 %all_gather.14 = bf16[128,512]{1,0:T(8,128)(2,1)S(1)} all-gather(bf16[32,512]{1,0:T(8,128)(2,1)S(1)} %reshape.217), channel_id=1, replica_groups=mesh['grp'=2,'tp'=4,'dp'=4] {'dp'}, dimensions={0}, use_global_device_ids=true | all-gather | bytes 163840 | tf_op jit(solution)/shard_map/all_gather | solution.py:118
  319.2 7.9 %mul.421 = f32[1,32,8,4096]{3,2,1,0:T(8,128)} reshape(f32[32,8,64,64]{3,2,1,0:T(8,128)} %get-tuple-element.20) | data formatting | bytes 8388608 | tf_op jit(solution)/shard_map/mul | solution.py:30
  327.1 7.9 %mul.423 = f32[1,32,8,4096]{3,2,1,0:T(8,128)} reshape(f32[32,8,64,64]{3,2,1,0:T(8,128)} %get-tuple-element.21) | data formatting | bytes 8388608 | tf_op jit(solution)/shard_map/mul | solution.py:31
  335.0 9.6 %multiply_add_fusion.1 = (f32[1,32,8,4096]{3,2,1,0:T(8,128)S(1)}, f32[1,32,8,4096]{3,2,1,0:T(8,128)S(1)}) fusion(f32[1,32,8,4096]{3,2,1,0:T(8,128)} %mul.419, f32[1,32,8,4096]{3,2,1,0:T(8,128)} %mul.417, f32[32,8]{1,0:T(8,128)S(1)} %copy.21, f32[2,32,8,4096]{3,2,1,0:T(8,128)} %param.14, f32[1,32,8,4096]{3,2,1,0:T(8,128)} %mul.423, ...), kind=kLoop, calls=%fused_computation.10 | loop fusion | flops 6291456 | bytes 33556480 | tf_op jit(solution)/shard_map/add | solution.py:30
  344.6 3.9 %pad_maximum_fusion = f32[2,32,8,4096]{3,2,1,0:T(8,128)} fusion(f32[1,32,8,4096]{3,2,1,0:T(8,128)S(1)} %get-tuple-element.15, f32[1,32,8,4096]{3,2,1,0:T(8,128)S(1)} %get-tuple-element.14), kind=kLoop, calls=%fused_computation | loop fusion | flops 2097152 | bytes 16777216 | tf_op jit(solution)/shard_map/stack | solution.py:133
  349.5 9.0 %all-reduce = (f32[32]{0:T(128)S(1)}, f32[32]{0:T(128)S(1)}) all-reduce(f32[32]{0:T(128)S(1)} %get-tuple-element.3, f32[32]{0:T(128)S(1)} %get-tuple-element.2), channel_id=1, replica_groups=mesh['grp'=2,'tp'=4,'dp'=4] {'dp'}, use_global_device_ids=true, to_apply=%region_27.28 | all-reduce | flops 64 | bytes 512 | tf_op jit(solution)/shard_map/psum | solution.py:130
  359.5 5.8 %all_gather.15 = bf16[128,1024]{1,0:T(8,128)(2,1)S(1)} all-gather(bf16[32,1024]{1,0:T(8,128)(2,1)S(1)} %add_convert_fusion), channel_id=1, replica_groups=mesh['grp'=2,'tp'=4,'dp'=4] {'tp'}, dimensions={0}, use_global_device_ids=true | all-gather | bytes 327680 | tf_op jit(solution)/shard_map/all_gather | solution.py:132
  (116 shorter events, 41.3 us)
Async XLA Ops:
  7.2 32.2 %reduce-scatter.45.cloned.1.call-start = ((), (), s32[]{:S(2)}) async-start(), calls=%async_computation.25 | async-start | bytes 40960
  10.0 41.9 %reduce-scatter.43.cloned.1.call-start = ((), (), s32[]{:S(2)}) async-start(), calls=%async_computation.24 | async-start | bytes 40960
  12.8 58.9 %reduce-scatter.23.cloned.1.call-start = ((), (), s32[]{:S(2)}) async-start(), calls=%async_computation.14 | async-start | bytes 163840 | tf_op jit(solution)/shard_map/reduce_scatter | solution.py:77
  15.1 76.3 %reduce-scatter.25.cloned.1.call-start = ((), (), s32[]{:S(2)}) async-start(), calls=%async_computation.15 | async-start | bytes 163840 | tf_op jit(solution)/shard_map/reduce_scatter | solution.py:80
  17.5 93.8 %reduce-scatter.27.cloned.1.call-start = ((), (), s32[]{:S(2)}) async-start(), calls=%async_computation.16 | async-start | bytes 163840 | tf_op jit(solution)/shard_map/reduce_scatter | solution.py:83
  19.8 111.7 %reduce-scatter.29.cloned.1.call-start = ((), (), s32[]{:S(2)}) async-start(), calls=%async_computation.17 | async-start | bytes 163840 | tf_op jit(solution)/shard_map/reduce_scatter | solution.py:86
  22.2 144.5 %reduce-scatter.31.cloned.1.call-start = ((), (), s32[]{:S(2)}) async-start(), calls=%async_computation.18 | async-start | bytes 327680 | tf_op jit(solution)/shard_map/reduce_scatter | solution.py:120
  102.1 46.3 %copy-start.1 = (f32[2,1024]{1,0:T(2,128)S(1)}, f32[2,1024]{1,0:T(2,128)}, u32[]{:S(2)}) copy-start(f32[2,1024]{1,0:T(2,128)} %param.24) | copy-start | bytes 24580
  102.1 46.3 %copy-start.2 = (f32[2,1024]{1,0:T(2,128)S(1)}, f32[2,1024]{1,0:T(2,128)}, u32[]{:S(2)}) copy-start(f32[2,1024]{1,0:T(2,128)} %param.25) | copy-start | bytes 24580
  102.1 64.6 %copy-start = (bf16[128,1024]{1,0:T(8,128)(2,1)S(1)}, bf16[128,1024]{1,0:T(8,128)(2,1)}, u32[]{:S(2)}) copy-start(bf16[128,1024]{1,0:T(8,128)(2,1)} %param.13) | copy-start | bytes 786436
  102.1 86.1 %copy-start.3 = (bf16[2,1024,512]{2,1,0:T(8,128)(2,1)S(1)}, bf16[2,1024,512]{2,1,0:T(8,128)(2,1)}, u32[]{:S(2)}) copy-start(bf16[2,1024,512]{2,1,0:T(8,128)(2,1)} %param.16) | copy-start | bytes 6291460
  148.3 76.1 %reduce-scatter.47.cloned.1.call-start = ((), (), s32[]{:S(2)}) async-start(), calls=%async_computation.26 | async-start | bytes 40960
  187.2 38.1 %reduce-scatter.49.cloned.1.call-start = ((), (), s32[]{:S(2)}) async-start(), calls=%async_computation.27 | async-start | bytes 40960
  188.2 55.1 %reduce-scatter.35.cloned.1.call-start = ((), (), s32[]{:S(2)}) async-start(), calls=%async_computation.20 | async-start | bytes 163840 | tf_op jit(solution)/shard_map/reduce_scatter | solution.py:80
  189.2 10.3 %copy-start.4 = (bf16[2,1024,512]{2,1,0:T(8,128)(2,1)S(1)}, bf16[2,1024,512]{2,1,0:T(8,128)(2,1)}, u32[]{:S(2)}) copy-start(bf16[2,1024,512]{2,1,0:T(8,128)(2,1)} %param.17) | copy-start | bytes 6291460
  189.3 73.9 %reduce-scatter.33.cloned.1.call-start = ((), (), s32[]{:S(2)}) async-start(), calls=%async_computation.19 | async-start | bytes 163840 | tf_op jit(solution)/shard_map/reduce_scatter | solution.py:77
  191.7 91.3 %reduce-scatter.37.cloned.1.call-start = ((), (), s32[]{:S(2)}) async-start(), calls=%async_computation.21 | async-start | bytes 163840 | tf_op jit(solution)/shard_map/reduce_scatter | solution.py:83
  200.6 102.9 %reduce-scatter.39.cloned.1.call-start = ((), (), s32[]{:S(2)}) async-start(), calls=%async_computation.22 | async-start | bytes 163840 | tf_op jit(solution)/shard_map/reduce_scatter | solution.py:86
  215.3 8.1 %copy-start.5 = (bf16[2,1024,512]{2,1,0:T(8,128)(2,1)S(1)}, bf16[2,1024,512]{2,1,0:T(8,128)(2,1)}, u32[]{:S(2)}) copy-start(bf16[2,1024,512]{2,1,0:T(8,128)(2,1)} %param.18) | copy-start | bytes 6291460
  224.3 124.2 %reduce-scatter.41.cloned.1.call-start = ((), (), s32[]{:S(2)}) async-start(), calls=%async_computation.23 | async-start | bytes 327680 | tf_op jit(solution)/shard_map/reduce_scatter | solution.py:120
  290.6 27.5 %copy-start.6 = (bf16[2,512,1024]{2,1,0:T(8,128)(2,1)S(1)}, bf16[2,512,1024]{2,1,0:T(8,128)(2,1)}, u32[]{:S(2)}) copy-start(bf16[2,512,1024]{2,1,0:T(8,128)(2,1)} %param.23) | copy-start | bytes 6291460
Sparse Core Ops, SparseCore 0:
  10.2 21.9 reduce-scatter.44
  34.4 17.3 reduce-scatter.42
  54.1 17.5 reduce-scatter.22
  73.8 17.6 reduce-scatter.24
  93.6 17.6 reduce-scatter.26
  113.9 17.6 reduce-scatter.28
  148.4 18.2 reduce-scatter.30
  187.4 16.4 reduce-scatter.46
  206.1 17.3 reduce-scatter.48
  225.6 17.6 reduce-scatter.34
  245.5 17.5 reduce-scatter.32
  265.3 17.6 reduce-scatter.36
  285.8 17.6 reduce-scatter.38
  319.3 18.2 reduce-scatter.40
where the time goes:
time: 375 us; the launch traced here: 372 us
  waiting for transfers between devices  133 us (35%)
  local copies, waits for them, and re-layouts  71.9 us (19%)
  matrix products  60.2 us (16%)
  blocking collectives  59.4 us (16%)
  other arithmetic  33.2 us (9%)
  between operations  14.3 us (4%)
    reduce_scatter x2, waiting for transfers between devices, per_device(): lax.psum_scatter(part_query.astype(jnp.bfloat16), 'dp', scatter_dimension...  37.9 us
    reduce_scatter x2, waiting for transfers between devices, per_device(): lax.psum_scatter(part_key.astype(jnp.bfloat16), 'dp', scatter_dimension=0...  35.8 us
    all_gather x2, blocking collectives, per_device(): gathered = lax.all_gather(read_flat, 'dp', axis=0, tiled=True)  27 us
    dot_general x2, matrix products, delta_step(): jnp.einsum('bhd,bhde->bhe', query_unit, matrix, precision=lax.Precision.H...  21.1 us
    psum x2, blocking collectives, per_device(): lax.psum((jnp.sum(combined, axis=1), jnp.sum(combined * combined, axis=1)...  20.9 us
    dot_general x2, matrix products, delta_step(): jnp.einsum('bhd,bhde->bhe', key_unit, matrix, precision=lax.Precision.HIG...  18.9 us
    reduce_scatter x2, waiting for transfers between devices, per_device(): lax.psum_scatter(jnp.dot(gathered, out_weight, preferred_element_type=jnp...  18.3 us
    reduce_scatter x2, waiting for transfers between devices, per_device(): lax.psum_scatter(part_value.astype(jnp.bfloat16), 'dp', scatter_dimension...  18.2 us
  transfers between devices with their start and end apart: 14, of which 10 were waited for; matrix products, arithmetic and copies ran while one was open for 41% of the time, Pallas kernels for 0%

commit v1 on v0

--- a/solution.py
+++ b/solution.py
@@ -1,6 +1,10 @@
+import functools
+
 import jax
 import jax.numpy as jnp
 from jax import lax
+from jax.experimental import pallas as pl
+from jax.experimental.pallas import tpu as pltpu
 from jax.sharding import PartitionSpec as P
 
 D = 4096
@@ -132,8 +136,445 @@
         stream = lax.all_gather(normed_rows, "tp", axis=0, tiled=True)
     return (stream, jnp.stack(states, axis=0))
 
+MESH = pl.DeviceIdType.MESH
+LANES = 128
+F32 = jnp.float32
+BF16 = jnp.bfloat16
+
+
+def fused_kernel(
+    n_dp,
+    n_tp,
+    hidden,
+    state,
+    w_query,
+    w_key,
+    w_value,
+    w_gate,
+    w_beta,
+    w_decay,
+    rate,
+    gain,
+    w_out,
+    post_gain,
+    post_bias,
+    hidden_out,
+    state_out,
+    stream,
+    st,
+    wp,
+    wbd,
+    wo,
+    psend,
+    precv,
+    bsend,
+    brecv,
+    ex,
+    qkx,
+    qk,
+    vg,
+    bt,
+    dc,
+    accq,
+    acck,
+    av,
+    wv,
+    rd,
+    rall,
+    msend,
+    mrecv,
+    ssend,
+    srecv,
+    load_sem,
+    out_sem,
+    p_ss,
+    p_rs,
+    r_ss,
+    r_rs,
+    m_ss,
+    m_rs,
+    s_ss,
+    s_rs,
+    g_ss,
+    g_rs,
+):
+    layers, seqs, heads, flat = st.shape
+    rows, feat = stream.shape[1:]
+    cols = wo.shape[1]
+    share = rows // n_tp
+    all_heads = wbd.shape[3]
+    hd = HEAD_DIM
+    tiles = flat // LANES
+    me_dp = lax.axis_index("dp")
+    me_tp = lax.axis_index("tp")
+
+    loads = {}
+
+    def load(name, src, dst, layer, index):
+        copy = pltpu.make_async_copy(src, dst, load_sem.at[layer, index])
+        copy.start()
+        loads[name, layer] = copy
+
+    first = pltpu.make_async_copy(hidden, stream.at[0], load_sem.at[0, 8])
+    first.start()
+    projections = (w_key, w_query, w_value, w_gate)
+    for layer in range(layers):
+        for j, w in enumerate(projections):
+            load(j, w.at[layer], wp.at[layer, j], layer, j)
+        load("b", w_beta.at[layer], wbd.at[layer, 0], layer, 4)
+        load("d", w_decay.at[layer], wbd.at[layer, 1], layer, 5)
+        load("s", state.at[layer], st.at[layer], layer, 6)
+        load("o", w_out.at[layer], wo.at[layer], layer, 7)
+
+    barrier = pltpu.get_barrier_semaphore()
+    for i in range(1, n_dp):
+        pl.semaphore_signal(
+            barrier, inc=1, device_id={"dp": lax.rem(me_dp + i, n_dp)}, device_id_type=MESH
+        )
+    for i in range(1, n_tp):
+        pl.semaphore_signal(
+            barrier, inc=1, device_id={"tp": lax.rem(me_tp + i, n_tp)}, device_id_type=MESH
+        )
+
+    chunk = 1024
+
+    def fill(n, carry):
+        at = pl.multiple_of(n * chunk, chunk)
+        row = lax.broadcasted_iota(jnp.int32, (LANES, chunk), 0)
+        col = lax.broadcasted_iota(jnp.int32, (LANES, chunk), 1) + at
+        hit = jnp.logical_and(col >= row * hd, col < (row + 1) * hd)
+        ex[:, pl.ds(at, chunk)] = jnp.where(hit, 1.0, 0.0).astype(BF16)
+        return carry
+
+    lax.fori_loop(0, 2 * flat // chunk, fill, 0)
+    pl.semaphore_wait(barrier, n_dp - 1 + n_tp - 1)
+
+    lane = lax.broadcasted_iota(jnp.int32, (seqs, LANES), 1)
+    low = lane < hd
+    lane_r = lax.broadcasted_iota(jnp.int32, (seqs * heads, LANES), 1)
+    low_r = lane_r < hd
+
+    def swap(x):
+        return pltpu.roll(x, hd, 1)
+
+    def to_rows(dst, a, b):
+        for h in range(heads):
+            sl = slice(h // 2 * LANES, h // 2 * LANES + LANES)
+            at, bt_ = a[:, sl], b[:, sl]
+            both = jnp.where(low, at, swap(bt_)) if h % 2 == 0 else jnp.where(low, swap(at), bt_)
+            dst[pl.ds(h, seqs, stride=heads), :] = both
+
+    sends = []
+
+    def remote(src, dst, ss, rs, axis, peer):
+        copy = pltpu.make_async_remote_copy(
+            src_ref=src,
+            dst_ref=dst,
+            send_sem=ss,
+            recv_sem=rs,
+            device_id={axis: peer},
+            device_id_type=MESH,
+        )
+        copy.start()
+        sends.append(copy)
+        return copy
+
+    first.wait()
+    gain_all = gain[...]
+    for layer in range(layers):
+        x = stream[layer]
+
+        def scatter(group, src, dst):
+            copies = []
+            for i in range(1, n_dp):
+                peer = lax.rem(me_dp + i, n_dp)
+                copies.append(
+                    remote(
+                        src.at[pl.ds(pl.multiple_of(peer * seqs, seqs), seqs)],
+                        dst.at[i - 1],
+                        p_ss.at[layer, group, i - 1],
+                        p_rs.at[layer, group, i - 1],
+                        "dp",
+                        peer,
+                    )
+                )
+            return copies
+
+        mine = pl.ds(pl.multiple_of(me_dp * seqs, seqs), seqs)
+        scattered = []
+        for j in range(4):
+            loads[j, layer].wait()
+            part = jnp.dot(x, wp[layer, j], preferred_element_type=F32)
+            psend[layer, j] = part.astype(BF16)
+            scattered.append(scatter(j, psend.at[layer, j], precv.at[layer, j]))
+            if j == 1:
+                loads["b", layer].wait()
+                loads["d", layer].wait()
+                pb = jnp.dot(x, wbd[layer, 0], preferred_element_type=F32)
+                pd = jnp.dot(x, wbd[layer, 1], preferred_element_type=F32)
+                pad = jnp.zeros((rows, LANES - 2 * all_heads), F32)
+                bsend[layer] = jnp.concatenate([pb, pd, pad], axis=1).astype(BF16)
+                scattered_b = scatter(4, bsend.at[layer], brecv.at[layer])
+
+        def total(copies, own, got):
+            acc = own.astype(F32)
+            for i, copy in enumerate(copies):
+                copy.wait_recv()
+                acc = acc + got[i].astype(F32)
+            return acc.astype(BF16).astype(F32)
+
+        def projected(j):
+            return total(scattered[j], psend[layer, j, mine, :], precv.at[layer, j])
+
+        keys = projected(0)
+        queries = projected(1)
+        to_rows(qk, queries, keys)
+        both = qk[...]
+        both_b = both.astype(BF16)
+
+        def expand(n, carry):
+            at = pl.multiple_of(n * chunk, chunk)
+            qkx[:, pl.ds(at, chunk)] = jnp.dot(
+                both_b, ex[:, pl.ds(at, chunk)], preferred_element_type=F32
+            )
+            return carry
+
+        lax.fori_loop(0, 2 * flat // chunk, expand, 0)
+        loads["s", layer].wait()
+
+        def reduce(s, carry):
+            at = pl.ds(pl.multiple_of(s * heads, heads), heads)
+            q_sums = [None, None]
+            k_sums = [None, None]
+            for t in range(tiles):
+                sl = slice(t * LANES, (t + 1) * LANES)
+                value = st[layer, s, :, sl]
+                qp = qkx[at, sl] * value
+                kp = qkx[at, flat + t * LANES : flat + (t + 1) * LANES] * value
+                p = t % 2
+                q_sums[p] = qp if q_sums[p] is None else q_sums[p] + qp
+                k_sums[p] = kp if k_sums[p] is None else k_sums[p] + kp
+            accq[at, :] = q_sums[0] + q_sums[1]
+            acck[at, :] = k_sums[0] + k_sums[1]
+            return carry
+
+        lax.fori_loop(0, seqs, reduce, 0)
+
+        bd = total(scattered_b, bsend[layer, mine, :], brecv.at[layer])
+        for h in range(heads):
+            head = me_tp * heads + h
+            beta_h = jnp.sum(jnp.where(lane == head, bd, 0.0), axis=1, keepdims=True)
+            decay_h = jnp.sum(jnp.where(lane == head + all_heads, bd, 0.0), axis=1, keepdims=True)
+            soft = jnp.maximum(decay_h, 0.0) + jnp.log1p(jnp.exp(-jnp.abs(decay_h)))
+            retain_h = jnp.exp(-rate[layer, h] * soft)
+            bt[pl.ds(h, seqs, stride=heads), :] = jnp.broadcast_to(
+                jax.nn.sigmoid(beta_h), (seqs, LANES)
+            )
+            av[pl.ds(h, seqs, stride=heads), :] = jnp.broadcast_to(retain_h, (seqs, LANES))
+
+        squares = both * both
+        q_sq = jnp.sum(jnp.where(low_r, squares, 0.0), axis=1, keepdims=True)
+        k_sq = jnp.sum(jnp.where(low_r, 0.0, squares), axis=1, keepdims=True)
+        q_dot_k = jnp.sum(jnp.where(low_r, both * swap(both), 0.0), axis=1, keepdims=True)
+        q_scale = lax.rsqrt(q_sq + 1e-06) * hd ** (-0.5)
+        k_scale = lax.rsqrt(k_sq + 1e-06)
+        q_read = accq[...]
+        q_read = q_read + swap(q_read)
+        k_read = acck[...]
+        k_read = (k_read + swap(k_read)) * k_scale
+        retain = av[...]
+
+        values = projected(2)
+        gates = projected(3)
+        to_rows(vg, values, gates)
+        vgr = vg[...]
+        vgs = swap(vgr)
+        v2 = jnp.where(low_r, vgr, vgs)
+        g2 = jnp.where(low_r, vgs, vgr)
+        write = bt[...] * k_scale * (v2 - retain * k_read)
+        wv[...] = write
+        o = q_scale * (retain * q_read + q_dot_k * write)
+        mean_sq = jnp.sum(o * o, axis=1, keepdims=True) / LANES
+        g_row = gain_all[layer : layer + 1, :]
+        g_row = jnp.concatenate([g_row, g_row], axis=1)
+        rd[...] = o * lax.rsqrt(mean_sq + 1e-05) * g_row * (g2 * jax.nn.sigmoid(g2))
+        for t in range(heads // 2):
+            even = rd[pl.ds(2 * t, seqs, stride=heads), :]
+            odd = rd[pl.ds(2 * t + 1, seqs, stride=heads), :]
+            rall[layer, mine, t * LANES : (t + 1) * LANES] = jnp.where(low, even, odd).astype(BF16)
+
+        gathered = []
+        for i in range(1, n_dp):
+            gathered.append(
+                remote(
+                    rall.at[layer, mine],
+                    rall.at[layer, mine],
+                    r_ss.at[layer, i - 1],
+                    r_rs.at[layer, i - 1],
+                    "dp",
+                    lax.rem(me_dp + i, n_dp),
+                )
+            )
+
+        def update(s, carry):
+            at = pl.ds(pl.multiple_of(s * heads, heads), heads)
+            keep = av[at, :]
+            add = wv[at, :]
+            for t in range(tiles):
+                sl = slice(t * LANES, (t + 1) * LANES)
+                key_t = qkx[at, flat + t * LANES : flat + (t + 1) * LANES]
+                st[layer, s, :, sl] = keep * st[layer, s, :, sl] + key_t * add
+            return carry
+
+        lax.fori_loop(0, seqs, update, 0)
+
+        loads["o", layer].wait()
+        for copy in gathered:
+            copy.wait_recv()
+        store = pltpu.make_async_copy(st.at[layer], state_out.at[layer], out_sem.at[layer])
+        store.start()
+        loads["store", layer] = store
+        msend[layer] = jnp.dot(rall[layer], wo[layer], preferred_element_type=F32).astype(BF16)
+        mixed = []
+        for i in range(1, n_tp):
+            peer = lax.rem(me_tp + i, n_tp)
+            mixed.append(
+                remote(
+                    msend.at[layer, pl.ds(pl.multiple_of(peer * share, share), share)],
+                    mrecv.at[layer, i - 1],
+                    m_ss.at[layer, i - 1],
+                    m_rs.at[layer, i - 1],
+                    "tp",
+                    peer,
+                )
+            )
+        part_rows = pl.ds(pl.multiple_of(me_tp * share, share), share)
+        combined = residual_scale * stream[layer, part_rows, :].astype(F32)
+        combined = combined + msend[layer, part_rows, :].astype(F32)
+        for i, copy in enumerate(mixed):
+            copy.wait_recv()
+            combined = combined + mrecv[layer, i].astype(F32)
+        s1 = jnp.sum(combined, axis=1, keepdims=True)
+        s2 = jnp.sum(combined * combined, axis=1, keepdims=True)
+        lane_s = lax.broadcasted_iota(jnp.int32, (share, LANES), 1)
+        sums = jnp.where(lane_s < hd, s1, s2)
+        ssend[layer] = sums
+        stats = []
+        for i in range(1, n_dp):
+            stats.append(
+                remote(
+                    ssend.at[layer],
+                    srecv.at[layer, i - 1],
+                    s_ss.at[layer, i - 1],
+                    s_rs.at[layer, i - 1],
+                    "dp",
+                    lax.rem(me_dp + i, n_dp),
+                )
+            )
+        for i, copy in enumerate(stats):
+            copy.wait_recv()
+            sums = sums + srecv[layer, i]
+        sums = sums / (feat * n_dp)
+        mean = sums[:, 0:1]
+        var = sums[:, hd : hd + 1] - mean * mean
+        normed = (combined - mean) * lax.rsqrt(var + 1e-05)
+        normed = normed * post_gain[layer : layer + 1, :] + post_bias[layer : layer + 1, :]
+        stream[layer + 1, part_rows, :] = normed.astype(BF16)
+        spread = []
+        for i in range(1, n_tp):
+            spread.append(
+                remote(
+                    stream.at[layer + 1, part_rows],
+                    stream.at[layer + 1, part_rows],
+                    g_ss.at[layer, i - 1],
+                    g_rs.at[layer, i - 1],
+                    "tp",
+                    lax.rem(me_tp + i, n_tp),
+                )
+            )
+        for copy in spread:
+            copy.wait_recv()
+
+    hidden_out[...] = stream[layers]
+    for copy in sends:
+        copy.wait_send()
+    for layer in range(layers):
+        loads["store", layer].wait()
+
+
+def fused_device(n_dp, n_tp, *args):
+    hidden, state, w_query = args[:3]
+    w_beta, out_weight = args[6], args[10]
+    layers, seqs, heads, flat = state.shape
+    rows, feat = hidden.shape
+    cols = w_query.shape[2]
+    all_heads = w_beta.shape[2]
+    share = rows // n_tp
+    r = seqs * heads
+    vm = pltpu.VMEM
+    dma = pltpu.SemaphoreType.DMA
+    whole = pl.BlockSpec(memory_space=pltpu.VMEM)
+    hbm = pl.BlockSpec(memory_space=pl.ANY)
+    row_tile = vm((r, LANES), F32)
+    return pl.pallas_call(
+        functools.partial(fused_kernel, n_dp, n_tp),
+        out_shape=(
+            jax.ShapeDtypeStruct(hidden.shape, BF16),
+            jax.ShapeDtypeStruct(state.shape, F32),
+        ),
+        in_specs=[hbm] * 8
+        + [pl.BlockSpec(memory_space=pltpu.SMEM), whole, hbm, whole, whole],
+        out_specs=(whole, hbm),
+        scratch_shapes=[
+            vm((layers + 1, rows, feat), BF16),
+            vm(state.shape, F32),
+            vm((layers, 4, feat, cols), BF16),
+            vm((layers, 2, feat, all_heads), BF16),
+            vm((layers, cols, feat), BF16),
+            vm((layers, 4, rows, cols), BF16),
+            vm((layers, 4, n_dp - 1, seqs, cols), BF16),
+            vm((layers, rows, LANES), BF16),
+            vm((layers, n_dp - 1, seqs, LANES), BF16),
+            vm((LANES, 2 * flat), BF16),
+            vm((r, 2 * flat), F32),
+        ]
+        + [row_tile] * 9
+        + [
+            vm((layers, rows, cols), BF16),
+            vm((layers, rows, feat), BF16),
+            vm((layers, n_tp - 1, share, feat), BF16),
+            vm((layers, share, LANES), F32),
+            vm((layers, n_dp - 1, share, LANES), F32),
+            dma((layers, 9)),
+            dma((layers,)),
+            dma((layers, 5, n_dp - 1)),
+            dma((layers, 5, n_dp - 1)),
+            dma((layers, n_dp - 1)),
+            dma((layers, n_dp - 1)),
+            dma((layers, n_tp - 1)),
+            dma((layers, n_tp - 1)),
+            dma((layers, n_dp - 1)),
+            dma((layers, n_dp - 1)),
+            dma((layers, n_tp - 1)),
+            dma((layers, n_tp - 1)),
+        ],
+        compiler_params=pltpu.CompilerParams(
+            collective_id=0, has_side_effects=True, vmem_limit_bytes=56 * 1024 * 1024
+        ),
+    )(*args)
+
 
 def solution(mesh):
+    n_dp, n_tp = mesh.shape["dp"], mesh.shape["tp"]
+
+    def body(*args):
+        hidden, state = args[:2]
+        heads = state.shape[2]
+        share = hidden.shape[0] // n_tp
+        if heads % 8 or share % 16 or state.shape[1] % 16 or hidden.shape[1] % LANES:
+            return per_device(*args)
+        return fused_device(n_dp, n_tp, *args)
+
     placed = (
         P("grp", "dp"),
         P(None, ("grp", "dp"), "tp", None),
@@ -150,7 +591,7 @@
         P(None, "dp"),
     )
     return jax.shard_map(
-        per_device,
+        body,
         mesh=mesh,
         in_specs=placed,
         out_specs=(P("grp", "dp"), P(None, ("grp", "dp"), "tp", None)),

time: 375 us -> 83.2 us (0.22)
  waiting for transfers between devices: 133 us -> 0 us
  Pallas kernels: 0 us -> 68.9 us
  matrix products: 60.2 us -> 0 us
  blocking collectives: 59.4 us -> 0 us
  local copies, waits for them, and re-layouts: 71.9 us -> 13.3 us
  other arithmetic: 33.2 us -> 0 us
  between operations: 14.3 us -> 0.64 us
    reduce_scatter x10 -> x0, waiting for transfers between devices: 121 us -> none  [the longest x2 37.9 us: per_device(): lax.psum_scatter(part_query.astype(jnp.bfloat16), 'dp', scatter_dimension...]
    pallas_call x0 -> x1, Pallas kernels: none -> 68.9 us  [fused_device(): pl.pallas_call(functools.partial(fused_kernel, n_dp, n_tp), out_shape=(ja...]
    dot_general x18 -> x0, matrix products: 60.2 us -> none  [the longest x2 21.1 us: delta_step(): jnp.einsum('bhd,bhde->bhe', query_unit, matrix, precision=lax.Precision.H...]
    all_gather x4 -> x0, blocking collectives: 38.5 us -> none  [the longest x2 27 us: per_device(): gathered = lax.all_gather(read_flat, 'dp', axis=0, tiled=True)]
    mul x5 -> x0, local copies, waits for them, and re-layouts: 32.6 us -> none  [the longest x2 15.9 us: delta_step(): beta_gate * key_unit[..., :, None] * values_f[..., None, :]]
    psum x2 -> x0, blocking collectives: 20.9 us -> none  [per_device(): lax.psum((jnp.sum(combined, axis=1), jnp.sum(combined * combined, axis=1)...]
    another operation x2 -> x0, local copies, waits for them, and re-layouts: 15.7 us -> none  [delta_step(): state_now.reshape(state_now.shape[0], state_now.shape[1], head_dim, head_...]
    mul x7 -> x0, other arithmetic: 14.7 us -> none  [the longest x4 13.8 us: delta_step(): beta_gate * key_unit[..., :, None] * readout[..., None, :]]
  transfers between devices with their start and end apart: 14 -> 0, of which waited for: 10 -> 0; matrix products, arithmetic and copies ran while one was open for 41% -> 0% of each run, Pallas kernels for 0% -> 0%
where the time goes in v1:
time: 83.2 us; the launch traced here: 82.9 us
  Pallas kernels  68.9 us (83%)
  local copies, waits for them, and re-layouts  13.3 us (16%)
    pallas_call x1, Pallas kernels, fused_device(): pl.pallas_call(functools.partial(fused_kernel, n_dp, n_tp), out_shape=(ja...  68.9 us
    unnamed x4, local copies, waits for them, and re-layouts  13.3 us

profile of v1, /device:TPU:0, one launch (start us, length us, event | category | flops | bytes accessed | tf_op | source)
XLA Modules:
  0.0 82.9 jit_solution(15846024237357590051)
XLA Ops:
  0.6 1.9 %copy.15.w_beta = bf16[2,1024,32]{2,1,0:T(8,128)(2,1)} copy(bf16[2,1024,32]{1,2,0:T(8,128)(2,1)} %param.19) | data formatting | bytes 262144 | tf_op args[6]
  2.5 2.0 %copy.16.w_decay = bf16[2,1024,32]{2,1,0:T(8,128)(2,1)} copy(bf16[2,1024,32]{1,2,0:T(8,128)(2,1)} %param.20) | data formatting | bytes 262144 | tf_op args[7]
  4.5 68.9 %shard_map.140 = (bf16[128,1024]{1,0:T(8,128)(2,1)}, f32[2,32,8,4096]{3,2,1,0:T(8,128)}) custom-call(bf16[128,1024]{1,0:T(8,128)(2,1)} %hidden.1, f32[2,32,8,4096]{3,2,1,0:T(8,128)} %state.1, bf16[2,1024,512]{2,1,0:T(8,128)(2,1)} %w_query.1, bf16[2,1024,512]{2,1,0:T(8,128)(2,1)} %w_key.1, bf16[2,1024,512]{2,1,0:T(8,128)(2,1)} %w_value.1, ...), custom_call_target="tpu_custom_call" | custom-call | tf_op jit(solution)/shard_map/pallas_call | solution.py:519
  73.4 1.7 %copy.19 = bf16[128,1024]{1,0:T(8,128)(2,1)} copy(bf16[128,1024]{1,0:T(8,128)(2,1)} %get-tuple-element.4) | data formatting | bytes 524288
  75.1 7.8 %copy.20 = f32[2,32,8,4096]{3,2,1,0:T(8,128)} copy(f32[2,32,8,4096]{3,2,1,0:T(8,128)} %get-tuple-element.5) | data formatting | bytes 16777216

commit v2 on v1

--- a/solution.py
+++ b/solution.py
@@ -1,4 +1,5 @@
 import functools
+import math
 
 import jax
 import jax.numpy as jnp
@@ -138,6 +139,8 @@
 
 MESH = pl.DeviceIdType.MESH
 LANES = 128
+VMEM_BYTES = 67043328
+VMEM_SLACK = 16 * 1024
 F32 = jnp.float32
 BF16 = jnp.bfloat16
 
@@ -153,15 +156,14 @@
     w_gate,
     w_beta,
     w_decay,
-    rate,
-    gain,
+    rate_in,
+    gain_in,
     w_out,
-    post_gain,
-    post_bias,
+    post_gain_in,
+    post_bias_in,
     hidden_out,
-    state_out,
+    st,
     stream,
-    st,
     wp,
     wbd,
     wo,
@@ -183,10 +185,13 @@
     rall,
     msend,
     mrecv,
-    ssend,
-    srecv,
+    raw,
+    sums,
+    rate,
+    gain,
+    post_gain,
+    post_bias,
     load_sem,
-    out_sem,
     p_ss,
     p_rs,
     r_ss,
@@ -202,7 +207,7 @@
     rows, feat = stream.shape[1:]
     cols = wo.shape[1]
     share = rows // n_tp
-    all_heads = wbd.shape[3]
+    all_heads = wbd.shape[2]
     hd = HEAD_DIM
     tiles = flat // LANES
     me_dp = lax.axis_index("dp")
@@ -218,23 +223,38 @@
     first = pltpu.make_async_copy(hidden, stream.at[0], load_sem.at[0, 8])
     first.start()
     projections = (w_key, w_query, w_value, w_gate)
-    for layer in range(layers):
+
+    def load_projections(layer):
         for j, w in enumerate(projections):
             load(j, w.at[layer], wp.at[layer, j], layer, j)
         load("b", w_beta.at[layer], wbd.at[layer, 0], layer, 4)
         load("d", w_decay.at[layer], wbd.at[layer, 1], layer, 5)
+
+    def load_rest(layer):
         load("s", state.at[layer], st.at[layer], layer, 6)
         load("o", w_out.at[layer], wo.at[layer], layer, 7)
 
+    load_projections(0)
+    small = []
+    for n, (src, dst) in enumerate(
+        (
+            (rate_in, rate),
+            (gain_in, gain),
+            (post_gain_in, post_gain),
+            (post_bias_in, post_bias),
+        )
+    ):
+        small.append(pltpu.make_async_copy(src, dst, load_sem.at[0, 9 + n]))
+        small[-1].start()
+
     barrier = pltpu.get_barrier_semaphore()
-    for i in range(1, n_dp):
-        pl.semaphore_signal(
-            barrier, inc=1, device_id={"dp": lax.rem(me_dp + i, n_dp)}, device_id_type=MESH
-        )
-    for i in range(1, n_tp):
-        pl.semaphore_signal(
-            barrier, inc=1, device_id={"tp": lax.rem(me_tp + i, n_tp)}, device_id_type=MESH
-        )
+    everyone = [(i, j) for i in range(n_tp) for j in range(n_dp) if i or j]
+
+    def peer_of(i, j):
+        return {"tp": lax.rem(me_tp + i, n_tp), "dp": lax.rem(me_dp + j, n_dp)}
+
+    for i, j in everyone:
+        pl.semaphore_signal(barrier, inc=1, device_id=peer_of(i, j), device_id_type=MESH)
 
     chunk = 1024
 
@@ -247,12 +267,15 @@
         return carry
 
     lax.fori_loop(0, 2 * flat // chunk, fill, 0)
-    pl.semaphore_wait(barrier, n_dp - 1 + n_tp - 1)
+    pl.semaphore_wait(barrier, len(everyone))
 
     lane = lax.broadcasted_iota(jnp.int32, (seqs, LANES), 1)
     low = lane < hd
     lane_r = lax.broadcasted_iota(jnp.int32, (seqs * heads, LANES), 1)
     low_r = lane_r < hd
+
+    def dot_t(a, b):
+        return lax.dot_general(a, b, (((1,), (1,)), ((), ())), preferred_element_type=F32)
 
     def swap(x):
         return pltpu.roll(x, hd, 1)
@@ -266,20 +289,23 @@
 
     sends = []
 
-    def remote(src, dst, ss, rs, axis, peer):
+    def remote(src, dst, ss, rs, axis, peer, start=True):
         copy = pltpu.make_async_remote_copy(
             src_ref=src,
             dst_ref=dst,
             send_sem=ss,
             recv_sem=rs,
-            device_id={axis: peer},
+            device_id=peer if axis is None else {axis: peer},
             device_id_type=MESH,
         )
-        copy.start()
+        if start:
+            copy.start()
         sends.append(copy)
         return copy
 
     first.wait()
+    for copy in small:
+        copy.wait()
     gain_all = gain[...]
     for layer in range(layers):
         x = stream[layer]
@@ -310,11 +336,14 @@
             if j == 1:
                 loads["b", layer].wait()
                 loads["d", layer].wait()
-                pb = jnp.dot(x, wbd[layer, 0], preferred_element_type=F32)
-                pd = jnp.dot(x, wbd[layer, 1], preferred_element_type=F32)
+                pb = dot_t(x, wbd[layer, 0])
+                pd = dot_t(x, wbd[layer, 1])
                 pad = jnp.zeros((rows, LANES - 2 * all_heads), F32)
                 bsend[layer] = jnp.concatenate([pb, pd, pad], axis=1).astype(BF16)
                 scattered_b = scatter(4, bsend.at[layer], brecv.at[layer])
+        load_rest(layer)
+        if layer + 1 < layers:
+            load_projections(layer + 1)
 
         def total(copies, own, got):
             acc = own.astype(F32)
@@ -429,12 +458,6 @@
         lax.fori_loop(0, seqs, update, 0)
 
         loads["o", layer].wait()
-        for copy in gathered:
-            copy.wait_recv()
-        store = pltpu.make_async_copy(st.at[layer], state_out.at[layer], out_sem.at[layer])
-        store.start()
-        loads["store", layer] = store
-        msend[layer] = jnp.dot(rall[layer], wo[layer], preferred_element_type=F32).astype(BF16)
         mixed = []
         for i in range(1, n_tp):
             peer = lax.rem(me_tp + i, n_tp)
@@ -446,90 +469,131 @@
                     m_rs.at[layer, i - 1],
                     "tp",
                     peer,
+                    start=False,
                 )
             )
+        for i in [0, 1] + list(range(n_dp - 1, 1, -1)):
+            block = lax.rem(me_dp + n_dp - i, n_dp)
+            if i:
+                gathered[i - 1].wait_recv()
+            at = pl.ds(pl.multiple_of(block * share, share), share)
+            msend[layer, at, :] = jnp.dot(
+                rall[layer, at, :], wo[layer], preferred_element_type=F32
+            ).astype(BF16)
+            step = lax.rem(block - me_tp + n_tp, n_tp)
+
+            @pl.when(step > 0)
+            def _():
+                pltpu.make_async_remote_copy(
+                    src_ref=msend.at[layer, at],
+                    dst_ref=mrecv.at[layer, step - 1],
+                    send_sem=m_ss.at[layer, step - 1],
+                    recv_sem=m_rs.at[layer, step - 1],
+                    device_id={"tp": block},
+                    device_id_type=MESH,
+                ).start()
+
         part_rows = pl.ds(pl.multiple_of(me_tp * share, share), share)
         combined = residual_scale * stream[layer, part_rows, :].astype(F32)
         combined = combined + msend[layer, part_rows, :].astype(F32)
         for i, copy in enumerate(mixed):
             copy.wait_recv()
             combined = combined + mrecv[layer, i].astype(F32)
+        eye = lax.broadcasted_iota(jnp.int32, (share, LANES), 0) == lax.broadcasted_iota(
+            jnp.int32, (share, LANES), 1
+        )
+
+        def as_row(column):
+            return jnp.sum(jnp.where(eye, column, 0.0), axis=0, keepdims=True)
+
+        def as_column(row):
+            return jnp.sum(jnp.where(eye, row, 0.0), axis=1, keepdims=True)
+
         s1 = jnp.sum(combined, axis=1, keepdims=True)
         s2 = jnp.sum(combined * combined, axis=1, keepdims=True)
-        lane_s = lax.broadcasted_iota(jnp.int32, (share, LANES), 1)
-        sums = jnp.where(lane_s < hd, s1, s2)
-        ssend[layer] = sums
-        stats = []
-        for i in range(1, n_dp):
-            stats.append(
-                remote(
-                    ssend.at[layer],
-                    srecv.at[layer, i - 1],
-                    s_ss.at[layer, i - 1],
-                    s_rs.at[layer, i - 1],
-                    "dp",
-                    lax.rem(me_dp + i, n_dp),
-                )
+        sums[layer, me_tp, me_dp, 0:1, :] = as_row(s1)
+        sums[layer, me_tp, me_dp, 1:2, :] = as_row(s2)
+        stats = {}
+        for i, j in everyone:
+            stats[i, j] = remote(
+                sums.at[layer, me_tp, me_dp],
+                sums.at[layer, me_tp, me_dp],
+                s_ss.at[layer, i, j],
+                s_rs.at[layer, i, j],
+                None,
+                peer_of(i, j),
             )
-        for i, copy in enumerate(stats):
-            copy.wait_recv()
-            sums = sums + srecv[layer, i]
-        sums = sums / (feat * n_dp)
-        mean = sums[:, 0:1]
-        var = sums[:, hd : hd + 1] - mean * mean
-        normed = (combined - mean) * lax.rsqrt(var + 1e-05)
-        normed = normed * post_gain[layer : layer + 1, :] + post_bias[layer : layer + 1, :]
-        stream[layer + 1, part_rows, :] = normed.astype(BF16)
+        raw[layer, part_rows, :] = combined.astype(BF16)
         spread = []
         for i in range(1, n_tp):
             spread.append(
                 remote(
-                    stream.at[layer + 1, part_rows],
-                    stream.at[layer + 1, part_rows],
+                    raw.at[layer, part_rows],
+                    raw.at[layer, part_rows],
                     g_ss.at[layer, i - 1],
                     g_rs.at[layer, i - 1],
                     "tp",
                     lax.rem(me_tp + i, n_tp),
                 )
             )
+        for copy in stats.values():
+            copy.wait_recv()
         for copy in spread:
             copy.wait_recv()
+        g_row = post_gain[layer : layer + 1, :]
+        b_row = post_bias[layer : layer + 1, :]
+        for t in range(n_tp):
+            both_sums = sums[layer, t, 0]
+            for d in range(1, n_dp):
+                both_sums = both_sums + sums[layer, t, d]
+            both_sums = both_sums / (feat * n_dp)
+            mean_row = both_sums[0:1, :]
+            rstd_row = lax.rsqrt(both_sums[1:2, :] - mean_row * mean_row + 1e-05)
+            at = slice(t * share, (t + 1) * share)
+            normed = (raw[layer, at, :].astype(F32) - as_column(mean_row)) * as_column(rstd_row)
+            stream[layer + 1, at, :] = (normed * g_row + b_row).astype(BF16)
 
     hidden_out[...] = stream[layers]
     for copy in sends:
         copy.wait_send()
-    for layer in range(layers):
-        loads["store", layer].wait()
+
+
+def drain_kernel(hidden, state, hidden_out, state_out, sem):
+    copies = [pltpu.make_async_copy(hidden, hidden_out, sem.at[0])]
+    for layer in range(state.shape[0]):
+        copies.append(
+            pltpu.make_async_copy(state.at[layer], state_out.at[layer], sem.at[layer + 1])
+        )
+    for copy in copies:
+        copy.start()
+    for copy in copies:
+        copy.wait()
 
 
 def fused_device(n_dp, n_tp, *args):
     hidden, state, w_query = args[:3]
-    w_beta, out_weight = args[6], args[10]
     layers, seqs, heads, flat = state.shape
     rows, feat = hidden.shape
     cols = w_query.shape[2]
-    all_heads = w_beta.shape[2]
+    all_heads = args[6].shape[2]
+    args = args[:6] + (args[6].swapaxes(1, 2), args[7].swapaxes(1, 2)) + args[8:]
     share = rows // n_tp
     r = seqs * heads
     vm = pltpu.VMEM
     dma = pltpu.SemaphoreType.DMA
     whole = pl.BlockSpec(memory_space=pltpu.VMEM)
     hbm = pl.BlockSpec(memory_space=pl.ANY)
+    grant = VMEM_BYTES - 4 * math.prod(state.shape) - 2 * math.prod(hidden.shape) - VMEM_SLACK
     row_tile = vm((r, LANES), F32)
-    return pl.pallas_call(
+    done = pl.pallas_call(
         functools.partial(fused_kernel, n_dp, n_tp),
-        out_shape=(
-            jax.ShapeDtypeStruct(hidden.shape, BF16),
-            jax.ShapeDtypeStruct(state.shape, F32),
-        ),
-        in_specs=[hbm] * 8
-        + [pl.BlockSpec(memory_space=pltpu.SMEM), whole, hbm, whole, whole],
-        out_specs=(whole, hbm),
+        out_shape=(vm(hidden.shape, BF16), vm(state.shape, F32)),
+        in_specs=[hbm] * 13,
+        out_specs=(whole, whole),
         scratch_shapes=[
             vm((layers + 1, rows, feat), BF16),
-            vm(state.shape, F32),
             vm((layers, 4, feat, cols), BF16),
-            vm((layers, 2, feat, all_heads), BF16),
+            vm((layers, 2, all_heads, feat), BF16),
             vm((layers, cols, feat), BF16),
             vm((layers, 4, rows, cols), BF16),
             vm((layers, 4, n_dp - 1, seqs, cols), BF16),
@@ -543,25 +607,39 @@
             vm((layers, rows, cols), BF16),
             vm((layers, rows, feat), BF16),
             vm((layers, n_tp - 1, share, feat), BF16),
-            vm((layers, share, LANES), F32),
-            vm((layers, n_dp - 1, share, LANES), F32),
-            dma((layers, 9)),
-            dma((layers,)),
+            vm((layers, rows, feat), BF16),
+            vm((layers, n_tp, n_dp, 2, LANES), F32),
+            pltpu.SMEM(args[8].shape, F32),
+            vm(args[9].shape, F32),
+            vm(args[11].shape, F32),
+            vm(args[12].shape, F32),
+            dma((layers, 13)),
             dma((layers, 5, n_dp - 1)),
             dma((layers, 5, n_dp - 1)),
             dma((layers, n_dp - 1)),
             dma((layers, n_dp - 1)),
             dma((layers, n_tp - 1)),
             dma((layers, n_tp - 1)),
-            dma((layers, n_dp - 1)),
-            dma((layers, n_dp - 1)),
+            dma((layers, n_tp, n_dp)),
+            dma((layers, n_tp, n_dp)),
             dma((layers, n_tp - 1)),
             dma((layers, n_tp - 1)),
         ],
         compiler_params=pltpu.CompilerParams(
-            collective_id=0, has_side_effects=True, vmem_limit_bytes=56 * 1024 * 1024
+            collective_id=0, has_side_effects=True, vmem_limit_bytes=grant
         ),
     )(*args)
+    return pl.pallas_call(
+        drain_kernel,
+        out_shape=(
+            jax.ShapeDtypeStruct(hidden.shape, BF16),
+            jax.ShapeDtypeStruct(state.shape, F32),
+        ),
+        in_specs=[whole, whole],
+        out_specs=(hbm, hbm),
+        scratch_shapes=[dma((layers + 1,))],
+        compiler_params=pltpu.CompilerParams(vmem_limit_bytes=1024 * 1024),
+    )(*done)
 
 
 def solution(mesh):
@@ -571,7 +649,7 @@
         hidden, state = args[:2]
         heads = state.shape[2]
         share = hidden.shape[0] // n_tp
-        if heads % 8 or share % 16 or state.shape[1] % 16 or hidden.shape[1] % LANES:
+        if n_dp != n_tp or heads % 8 or share % 16 or state.shape[1] % 16 or hidden.shape[1] % LANES:
             return per_device(*args)
         return fused_device(n_dp, n_tp, *args)
 

time: 83.2 us -> 67 us (0.81)
  local copies, waits for them, and re-layouts: 13.3 us -> 0 us
  Pallas kernels: 68.9 us -> 66.2 us
    unnamed x4 -> x0, local copies, waits for them, and re-layouts: 13.3 us -> none
    pallas_call x1 -> x2, Pallas kernels: 68.9 us -> 66.2 us  [the longest x1 62.7 us: fused_device(): pl.pallas_call(functools.partial(fused_kernel, n_dp, n_tp), out_shape=(vm...]
where the time goes in v2:
time: 67 us; the launch traced here: 66.8 us
  Pallas kernels  66.2 us (99%)
    pallas_call x1, Pallas kernels, fused_device(): pl.pallas_call(functools.partial(fused_kernel, n_dp, n_tp), out_shape=(vm...  62.7 us
    pallas_call x1, Pallas kernels, fused_device(): pl.pallas_call(drain_kernel, out_shape=(jax.ShapeDtypeStruct(hidden.shape...  3.51 us

profile of v2, /device:TPU:0, one launch (start us, length us, event | category | flops | bytes accessed | tf_op | source)
XLA Modules:
  0.0 66.8 jit_solution(1117910655657216319)
XLA Ops:
  0.6 62.7 %shard_map.140 = (bf16[128,1024]{1,0:T(8,128)(2,1)S(1)}, f32[2,32,8,4096]{3,2,1,0:T(8,128)S(1)}) custom-call(bf16[128,1024]{1,0:T(8,128)(2,1)} %hidden.1, f32[2,32,8,4096]{3,2,1,0:T(8,128)} %state.1, bf16[2,1024,512]{2,1,0:T(8,128)(2,1)} %w_query.1, bf16[2,1024,512]{2,1,0:T(8,128)(2,1)} %w_key.1, bf16[2,1024,512]{2,1,0:T(8,128)(2,1)} %w_value.1, ...), custom_call_target="tpu_custom_call" | custom-call | tf_op jit(solution)/shard_map/pallas_call | solution.py:588
  63.3 3.5 %shard_map.141 = (bf16[128,1024]{1,0:T(8,128)(2,1)}, f32[2,32,8,4096]{3,2,1,0:T(8,128)}) custom-call(bf16[128,1024]{1,0:T(8,128)(2,1)S(1)} %get-tuple-element.4.hidden, f32[2,32,8,4096]{3,2,1,0:T(8,128)S(1)} %get-tuple-element.5.state), custom_call_target="tpu_custom_call" | custom-call | tf_op jit(solution)/shard_map/pallas_call | solution.py:632

commit v3 on v2

--- a/solution.py
+++ b/solution.py
@@ -140,6 +140,9 @@
 MESH = pl.DeviceIdType.MESH
 LANES = 128
 VMEM_BYTES = 67043328
+HALVES = 2
+START = (0, 1)
+ORDER = (0, 1, 0, 1, 0, 1, 0, 1)
 VMEM_SLACK = 16 * 1024
 F32 = jnp.float32
 BF16 = jnp.bfloat16
@@ -192,6 +195,7 @@
     post_gain,
     post_bias,
     load_sem,
+    first_sem,
     p_ss,
     p_rs,
     r_ss,
@@ -203,8 +207,9 @@
     g_ss,
     g_rs,
 ):
-    layers, seqs, heads, flat = st.shape
-    rows, feat = stream.shape[1:]
+    layers, all_seqs, heads, flat = st.shape
+    halves, _, rows, feat = stream.shape
+    seqs = all_seqs // halves
     cols = wo.shape[1]
     share = rows // n_tp
     all_heads = wbd.shape[2]
@@ -220,8 +225,17 @@
         copy.start()
         loads[name, layer] = copy
 
-    first = pltpu.make_async_copy(hidden, stream.at[0], load_sem.at[0, 8])
-    first.start()
+    first = []
+    for h in range(halves):
+        for d in range(n_dp):
+            first.append(
+                pltpu.make_async_copy(
+                    hidden.at[pl.ds(d * all_seqs + h * seqs, seqs)],
+                    stream.at[h, 0, pl.ds(d * seqs, seqs)],
+                    first_sem.at[h, d],
+                )
+            )
+            first[-1].start()
     projections = (w_key, w_query, w_value, w_gate)
 
     def load_projections(layer):
@@ -303,12 +317,13 @@
         sends.append(copy)
         return copy
 
-    first.wait()
+    for copy in first:
+        copy.wait()
     for copy in small:
         copy.wait()
     gain_all = gain[...]
-    for layer in range(layers):
-        x = stream[layer]
+    def block(layer, half):
+        x = stream[half, layer]
 
         def scatter(group, src, dst):
             copies = []
@@ -318,8 +333,8 @@
                     remote(
                         src.at[pl.ds(pl.multiple_of(peer * seqs, seqs), seqs)],
                         dst.at[i - 1],
-                        p_ss.at[layer, group, i - 1],
-                        p_rs.at[layer, group, i - 1],
+                        p_ss.at[half, layer, group, i - 1],
+                        p_rs.at[half, layer, group, i - 1],
                         "dp",
                         peer,
                     )
@@ -329,21 +344,26 @@
         mine = pl.ds(pl.multiple_of(me_dp * seqs, seqs), seqs)
         scattered = []
         for j in range(4):
-            loads[j, layer].wait()
+            if half == 0:
+                loads[j, layer].wait()
             part = jnp.dot(x, wp[layer, j], preferred_element_type=F32)
-            psend[layer, j] = part.astype(BF16)
-            scattered.append(scatter(j, psend.at[layer, j], precv.at[layer, j]))
+            psend[half, layer, j] = part.astype(BF16)
+            scattered.append(scatter(j, psend.at[half, layer, j], precv.at[half, layer, j]))
             if j == 1:
-                loads["b", layer].wait()
-                loads["d", layer].wait()
+                if half == 0:
+                    loads["b", layer].wait()
+                if half == 0:
+                    loads["d", layer].wait()
                 pb = dot_t(x, wbd[layer, 0])
                 pd = dot_t(x, wbd[layer, 1])
                 pad = jnp.zeros((rows, LANES - 2 * all_heads), F32)
-                bsend[layer] = jnp.concatenate([pb, pd, pad], axis=1).astype(BF16)
-                scattered_b = scatter(4, bsend.at[layer], brecv.at[layer])
-        load_rest(layer)
-        if layer + 1 < layers:
-            load_projections(layer + 1)
+                bsend[half, layer] = jnp.concatenate([pb, pd, pad], axis=1).astype(BF16)
+                scattered_b = scatter(4, bsend.at[half, layer], brecv.at[half, layer])
+        if half == 0:
+            load_rest(layer)
+            if layer + 1 < layers:
+                load_projections(layer + 1)
+        yield
 
         def total(copies, own, got):
             acc = own.astype(F32)
@@ -353,7 +373,7 @@
             return acc.astype(BF16).astype(F32)
 
         def projected(j):
-            return total(scattered[j], psend[layer, j, mine, :], precv.at[layer, j])
+            return total(scattered[j], psend[half, layer, j, mine, :], precv.at[half, layer, j])
 
         keys = projected(0)
         queries = projected(1)
@@ -369,7 +389,8 @@
             return carry
 
         lax.fori_loop(0, 2 * flat // chunk, expand, 0)
-        loads["s", layer].wait()
+        if half == 0:
+            loads["s", layer].wait()
 
         def reduce(s, carry):
             at = pl.ds(pl.multiple_of(s * heads, heads), heads)
@@ -377,7 +398,7 @@
             k_sums = [None, None]
             for t in range(tiles):
                 sl = slice(t * LANES, (t + 1) * LANES)
-                value = st[layer, s, :, sl]
+                value = st[layer, half * seqs + s, :, sl]
                 qp = qkx[at, sl] * value
                 kp = qkx[at, flat + t * LANES : flat + (t + 1) * LANES] * value
                 p = t % 2
@@ -389,7 +410,7 @@
 
         lax.fori_loop(0, seqs, reduce, 0)
 
-        bd = total(scattered_b, bsend[layer, mine, :], brecv.at[layer])
+        bd = total(scattered_b, bsend[half, layer, mine, :], brecv.at[half, layer])
         for h in range(heads):
             head = me_tp * heads + h
             beta_h = jnp.sum(jnp.where(lane == head, bd, 0.0), axis=1, keepdims=True)
@@ -430,16 +451,16 @@
         for t in range(heads // 2):
             even = rd[pl.ds(2 * t, seqs, stride=heads), :]
             odd = rd[pl.ds(2 * t + 1, seqs, stride=heads), :]
-            rall[layer, mine, t * LANES : (t + 1) * LANES] = jnp.where(low, even, odd).astype(BF16)
+            rall[half, layer, mine, t * LANES : (t + 1) * LANES] = jnp.where(low, even, odd).astype(BF16)
 
         gathered = []
         for i in range(1, n_dp):
             gathered.append(
                 remote(
-                    rall.at[layer, mine],
-                    rall.at[layer, mine],
-                    r_ss.at[layer, i - 1],
-                    r_rs.at[layer, i - 1],
+                    rall.at[half, layer, mine],
+                    rall.at[half, layer, mine],
+                    r_ss.at[half, layer, i - 1],
+                    r_rs.at[half, layer, i - 1],
                     "dp",
                     lax.rem(me_dp + i, n_dp),
                 )
@@ -452,21 +473,23 @@
             for t in range(tiles):
                 sl = slice(t * LANES, (t + 1) * LANES)
                 key_t = qkx[at, flat + t * LANES : flat + (t + 1) * LANES]
-                st[layer, s, :, sl] = keep * st[layer, s, :, sl] + key_t * add
+                st[layer, half * seqs + s, :, sl] = keep * st[layer, half * seqs + s, :, sl] + key_t * add
             return carry
 
         lax.fori_loop(0, seqs, update, 0)
-
-        loads["o", layer].wait()
+        yield
+
+        if half == 0:
+            loads["o", layer].wait()
         mixed = []
         for i in range(1, n_tp):
             peer = lax.rem(me_tp + i, n_tp)
             mixed.append(
                 remote(
-                    msend.at[layer, pl.ds(pl.multiple_of(peer * share, share), share)],
-                    mrecv.at[layer, i - 1],
-                    m_ss.at[layer, i - 1],
-                    m_rs.at[layer, i - 1],
+                    msend.at[half, layer, pl.ds(pl.multiple_of(peer * share, share), share)],
+                    mrecv.at[half, layer, i - 1],
+                    m_ss.at[half, layer, i - 1],
+                    m_rs.at[half, layer, i - 1],
                     "tp",
                     peer,
                     start=False,
@@ -477,28 +500,29 @@
             if i:
                 gathered[i - 1].wait_recv()
             at = pl.ds(pl.multiple_of(block * share, share), share)
-            msend[layer, at, :] = jnp.dot(
-                rall[layer, at, :], wo[layer], preferred_element_type=F32
+            msend[half, layer, at, :] = jnp.dot(
+                rall[half, layer, at, :], wo[layer], preferred_element_type=F32
             ).astype(BF16)
             step = lax.rem(block - me_tp + n_tp, n_tp)
 
             @pl.when(step > 0)
             def _():
                 pltpu.make_async_remote_copy(
-                    src_ref=msend.at[layer, at],
-                    dst_ref=mrecv.at[layer, step - 1],
-                    send_sem=m_ss.at[layer, step - 1],
-                    recv_sem=m_rs.at[layer, step - 1],
+                    src_ref=msend.at[half, layer, at],
+                    dst_ref=mrecv.at[half, layer, step - 1],
+                    send_sem=m_ss.at[half, layer, step - 1],
+                    recv_sem=m_rs.at[half, layer, step - 1],
                     device_id={"tp": block},
                     device_id_type=MESH,
                 ).start()
 
+        yield
         part_rows = pl.ds(pl.multiple_of(me_tp * share, share), share)
-        combined = residual_scale * stream[layer, part_rows, :].astype(F32)
-        combined = combined + msend[layer, part_rows, :].astype(F32)
+        combined = residual_scale * stream[half, layer, part_rows, :].astype(F32)
+        combined = combined + msend[half, layer, part_rows, :].astype(F32)
         for i, copy in enumerate(mixed):
             copy.wait_recv()
-            combined = combined + mrecv[layer, i].astype(F32)
+            combined = combined + mrecv[half, layer, i].astype(F32)
         eye = lax.broadcasted_iota(jnp.int32, (share, LANES), 0) == lax.broadcasted_iota(
             jnp.int32, (share, LANES), 1
         )
@@ -511,31 +535,32 @@
 
         s1 = jnp.sum(combined, axis=1, keepdims=True)
         s2 = jnp.sum(combined * combined, axis=1, keepdims=True)
-        sums[layer, me_tp, me_dp, 0:1, :] = as_row(s1)
-        sums[layer, me_tp, me_dp, 1:2, :] = as_row(s2)
+        sums[half, layer, me_tp, me_dp, 0:1, :] = as_row(s1)
+        sums[half, layer, me_tp, me_dp, 1:2, :] = as_row(s2)
         stats = {}
         for i, j in everyone:
             stats[i, j] = remote(
-                sums.at[layer, me_tp, me_dp],
-                sums.at[layer, me_tp, me_dp],
-                s_ss.at[layer, i, j],
-                s_rs.at[layer, i, j],
+                sums.at[half, layer, me_tp, me_dp],
+                sums.at[half, layer, me_tp, me_dp],
+                s_ss.at[half, layer, i, j],
+                s_rs.at[half, layer, i, j],
                 None,
                 peer_of(i, j),
             )
-        raw[layer, part_rows, :] = combined.astype(BF16)
+        raw[half, layer, part_rows, :] = combined.astype(BF16)
         spread = []
         for i in range(1, n_tp):
             spread.append(
                 remote(
-                    raw.at[layer, part_rows],
-                    raw.at[layer, part_rows],
-                    g_ss.at[layer, i - 1],
-                    g_rs.at[layer, i - 1],
+                    raw.at[half, layer, part_rows],
+                    raw.at[half, layer, part_rows],
+                    g_ss.at[half, layer, i - 1],
+                    g_rs.at[half, layer, i - 1],
                     "tp",
                     lax.rem(me_tp + i, n_tp),
                 )
             )
+        yield
         for copy in stats.values():
             copy.wait_recv()
         for copy in spread:
@@ -543,17 +568,28 @@
         g_row = post_gain[layer : layer + 1, :]
         b_row = post_bias[layer : layer + 1, :]
         for t in range(n_tp):
-            both_sums = sums[layer, t, 0]
+            both_sums = sums[half, layer, t, 0]
             for d in range(1, n_dp):
-                both_sums = both_sums + sums[layer, t, d]
+                both_sums = both_sums + sums[half, layer, t, d]
             both_sums = both_sums / (feat * n_dp)
             mean_row = both_sums[0:1, :]
             rstd_row = lax.rsqrt(both_sums[1:2, :] - mean_row * mean_row + 1e-05)
             at = slice(t * share, (t + 1) * share)
-            normed = (raw[layer, at, :].astype(F32) - as_column(mean_row)) * as_column(rstd_row)
-            stream[layer + 1, at, :] = (normed * g_row + b_row).astype(BF16)
-
-    hidden_out[...] = stream[layers]
+            normed = (raw[half, layer, at, :].astype(F32) - as_column(mean_row)) * as_column(rstd_row)
+            stream[half, layer + 1, at, :] = (normed * g_row + b_row).astype(BF16)
+
+    def run(half):
+        for layer in range(layers):
+            yield from block(layer, half)
+
+    runs = [run(half) for half in range(halves)]
+    for half in START + ORDER * layers:
+        next(runs[half], None)
+
+    for h in range(halves):
+        for d in range(n_dp):
+            at = d * all_seqs + h * seqs
+            hidden_out[at : at + seqs, :] = stream[h, layers, d * seqs : (d + 1) * seqs, :]
     for copy in sends:
         copy.wait_send()
 
@@ -573,7 +609,8 @@
 def fused_device(n_dp, n_tp, *args):
     hidden, state, w_query = args[:3]
     layers, seqs, heads, flat = state.shape
-    rows, feat = hidden.shape
+    rows, feat = hidden.shape[0] // HALVES, hidden.shape[1]
+    seqs = seqs // HALVES
     cols = w_query.shape[2]
     all_heads = args[6].shape[2]
     args = args[:6] + (args[6].swapaxes(1, 2), args[7].swapaxes(1, 2)) + args[8:]
@@ -591,39 +628,40 @@
         in_specs=[hbm] * 13,
         out_specs=(whole, whole),
         scratch_shapes=[
-            vm((layers + 1, rows, feat), BF16),
+            vm((HALVES, layers + 1, rows, feat), BF16),
             vm((layers, 4, feat, cols), BF16),
             vm((layers, 2, all_heads, feat), BF16),
             vm((layers, cols, feat), BF16),
-            vm((layers, 4, rows, cols), BF16),
-            vm((layers, 4, n_dp - 1, seqs, cols), BF16),
-            vm((layers, rows, LANES), BF16),
-            vm((layers, n_dp - 1, seqs, LANES), BF16),
+            vm((HALVES, layers, 4, rows, cols), BF16),
+            vm((HALVES, layers, 4, n_dp - 1, seqs, cols), BF16),
+            vm((HALVES, layers, rows, LANES), BF16),
+            vm((HALVES, layers, n_dp - 1, seqs, LANES), BF16),
             vm((LANES, 2 * flat), BF16),
             vm((r, 2 * flat), F32),
         ]
         + [row_tile] * 9
         + [
-            vm((layers, rows, cols), BF16),
-            vm((layers, rows, feat), BF16),
-            vm((layers, n_tp - 1, share, feat), BF16),
-            vm((layers, rows, feat), BF16),
-            vm((layers, n_tp, n_dp, 2, LANES), F32),
+            vm((HALVES, layers, rows, cols), BF16),
+            vm((HALVES, layers, rows, feat), BF16),
+            vm((HALVES, layers, n_tp - 1, share, feat), BF16),
+            vm((HALVES, layers, rows, feat), BF16),
+            vm((HALVES, layers, n_tp, n_dp, 2, LANES), F32),
             pltpu.SMEM(args[8].shape, F32),
             vm(args[9].shape, F32),
             vm(args[11].shape, F32),
             vm(args[12].shape, F32),
             dma((layers, 13)),
-            dma((layers, 5, n_dp - 1)),
-            dma((layers, 5, n_dp - 1)),
-            dma((layers, n_dp - 1)),
-            dma((layers, n_dp - 1)),
-            dma((layers, n_tp - 1)),
-            dma((layers, n_tp - 1)),
-            dma((layers, n_tp, n_dp)),
-            dma((layers, n_tp, n_dp)),
-            dma((layers, n_tp - 1)),
-            dma((layers, n_tp - 1)),
+            dma((HALVES, n_dp)),
+            dma((HALVES, layers, 5, n_dp - 1)),
+            dma((HALVES, layers, 5, n_dp - 1)),
+            dma((HALVES, layers, n_dp - 1)),
+            dma((HALVES, layers, n_dp - 1)),
+            dma((HALVES, layers, n_tp - 1)),
+            dma((HALVES, layers, n_tp - 1)),
+            dma((HALVES, layers, n_tp, n_dp)),
+            dma((HALVES, layers, n_tp, n_dp)),
+            dma((HALVES, layers, n_tp - 1)),
+            dma((HALVES, layers, n_tp - 1)),
         ],
         compiler_params=pltpu.CompilerParams(
             collective_id=0, has_side_effects=True, vmem_limit_bytes=grant
@@ -649,7 +687,7 @@
         hidden, state = args[:2]
         heads = state.shape[2]
         share = hidden.shape[0] // n_tp
-        if n_dp != n_tp or heads % 8 or share % 16 or state.shape[1] % 16 or hidden.shape[1] % LANES:
+        if n_dp != n_tp or heads % 8 or share % (16 * HALVES) or hidden.shape[1] % LANES:
             return per_device(*args)
         return fused_device(n_dp, n_tp, *args)
 

time: 67 us -> 66.2 us (0.988)
  Pallas kernels: 66.2 us -> 65.4 us
    pallas_call x1, Pallas kernels: 62.7 us -> 61.9 us  [fused_device(): pl.pallas_call(functools.partial(fused_kernel, n_dp, n_tp), out_shape=(vm...]
where the time goes in v3:
time: 66.2 us; the launch traced here: 66 us
  Pallas kernels  65.4 us (99%)
    pallas_call x1, Pallas kernels, fused_device(): pl.pallas_call(functools.partial(fused_kernel, n_dp, n_tp), out_shape=(vm...  61.9 us
    pallas_call x1, Pallas kernels, fused_device(): pl.pallas_call(drain_kernel, out_shape=(jax.ShapeDtypeStruct(hidden.shape...  3.51 us

profile of v3, /device:TPU:0, one launch (start us, length us, event | category | flops | bytes accessed | tf_op | source)
XLA Modules:
  0.0 66.0 jit_solution(4004494263310551434)
XLA Ops:
  0.6 61.9 %shard_map.140 = (bf16[128,1024]{1,0:T(8,128)(2,1)S(1)}, f32[2,32,8,4096]{3,2,1,0:T(8,128)S(1)}) custom-call(bf16[128,1024]{1,0:T(8,128)(2,1)} %hidden.1, f32[2,32,8,4096]{3,2,1,0:T(8,128)} %state.1, bf16[2,1024,512]{2,1,0:T(8,128)(2,1)} %w_query.1, bf16[2,1024,512]{2,1,0:T(8,128)(2,1)} %w_key.1, bf16[2,1024,512]{2,1,0:T(8,128)(2,1)} %w_value.1, ...), custom_call_target="tpu_custom_call" | custom-call | tf_op jit(solution)/shard_map/pallas_call | solution.py:625
  62.5 3.5 %shard_map.141 = (bf16[128,1024]{1,0:T(8,128)(2,1)}, f32[2,32,8,4096]{3,2,1,0:T(8,128)}) custom-call(bf16[128,1024]{1,0:T(8,128)(2,1)S(1)} %get-tuple-element.4.hidden, f32[2,32,8,4096]{3,2,1,0:T(8,128)S(1)} %get-tuple-element.5.state), custom_call_target="tpu_custom_call" | custom-call | tf_op jit(solution)/shard_map/pallas_call | solution.py:670
